TPU v7x, 32 devices: a whole 2x2x4 slice. The times are simulated.
32 devices in a mesh: sp: 4 (over z), fs: 4 (over y, x), tp: 2 (over core).
Axes of the slice: x: 2, y: 2, z: 4, core: 2. Of those that a mesh axis runs over, the one named last changes fastest.
Arguments:
- tokens: bfloat16 [512, 2048], P(('sp', 'fs', 'tp')), may hold values from -16 to 16
- in_gain: float32 [2048], replicated, may hold values from 0.1 to 1.9
- ret_query: bfloat16 [2048, 1024], P(None, ('fs', 'tp')), may hold values from -0.125 to 0.125
- ret_key: bfloat16 [2048, 1024], P(None, ('fs', 'tp')), may hold values from -0.125 to 0.125
- ret_value: bfloat16 [2048, 1024], P(None, ('fs', 'tp')), may hold values from -0.125 to 0.125
- decay_log: float32 [8, 512], P(('fs', 'tp'), 'sp'), may hold values from -1 to 0
- init_state: bfloat16 [8, 128, 128], P(('fs', 'tp')), may hold values from -24 to 24
- ret_gain: float32 [1024], P(('fs', 'tp')), may hold values from 0.1 to 1.9
- diff_query: bfloat16 [2, 2048, 512], P(None, None, ('fs', 'tp')), may hold values from -1 to 1
- diff_key: bfloat16 [2, 2048, 512], P(None, None, ('fs', 'tp')), may hold values from -1 to 1
- diff_value: bfloat16 [2048, 1024], P(None, ('fs', 'tp')), may hold values from -0.125 to 0.125
- diff_lambda: float32 [8], P(('fs', 'tp')), may hold values from 0.3 to 0.8
- diff_gain: float32 [1024], P(('fs', 'tp')), may hold values from 0.1 to 1.9
- out_weight: bfloat16 [2, 1024, 2048], P(None, ('fs', 'tp'), 'sp'), may hold values from -0.125 to 0.125
Outputs:
- mixed: bfloat16 [512, 2048], P(('sp', 'fs', 'tp'))
All inputs are finite; a program needn't handle non-finite values.
Results may differ from a plain program's by a relative error of at most 0.017.
Values may be sent and summed in bfloat16 or wider, within the bound.
A program may use at most 64 MiB of HBM per device.

v0:
```python
import functools

import jax
import jax.numpy as jnp
from jax import lax
from jax.experimental import pallas as pl
from jax.experimental.pallas import tpu as pltpu
from jax.sharding import PartitionSpec as P

EPS = 1e-06
HUGE = 1e30
TOKEN_CHUNKS = 1
f32 = jnp.float32
bf16 = jnp.bfloat16


def kernel(
    sizes,
    tokens,
    in_gain,
    ret_query,
    ret_key,
    ret_value,
    decay_log,
    init_state,
    ret_gain,
    diff_query,
    diff_key,
    diff_value,
    diff_lambda,
    diff_gain,
    out_weight,
    out,
    x_all,
    w_all,
    w_pair,
    tok_in,
    gain_in,
    decay_in,
    init_in,
    ret_gain_in,
    lambda_in,
    diff_gain_in,
    kv,
    st,
    wo,
    part,
    sib,
    red,
    rcv,
    load_sem,
    tok_send,
    tok_recv,
    fwd_send,
    kv_send,
    kv_recv,
    st_send,
    st_recv,
    wo_send,
    wo_recv,
    sib_send,
    sib_recv,
    rs_send,
    rs_recv,
):
    n_sp, n_fs, n_tp, ring = sizes
    own_rows, width = tokens.shape
    rows = own_rows * n_fs * n_tp
    head = ret_query.shape[1]
    maps = diff_query.shape[0] // 2
    sp, fs, tp = lax.axis_index("sp"), lax.axis_index("fs"), lax.axis_index("tp")
    half = max(n_fs // 2, 1)
    fs_peers = []
    for d in range(1, n_fs):
        if n_fs % 2 == 0:
            fs_peers.append(
                lax.rem(lax.div(fs, 2) + d // 2, half) * 2 + lax.rem(lax.rem(fs, 2) + d % 2, 2)
            )
        else:
            fs_peers.append(lax.rem(fs + d, n_fs))
    tp_peers = [lax.rem(tp + d, n_tp) for d in range(1, n_tp)]

    def remote(src, dst, send, recv, s, f, t):
        return pltpu.make_async_remote_copy(
            src_ref=src,
            dst_ref=dst,
            send_sem=send,
            recv_sem=recv,
            device_id=(s, f, t),
            device_id_type=pl.DeviceIdType.MESH,
        )

    barrier = pltpu.get_barrier_semaphore()

    def greet(s, f, t):
        pl.semaphore_signal(
            barrier, inc=1, device_id=(s, f, t), device_id_type=pl.DeviceIdType.MESH
        )

    for f in fs_peers:
        greet(sp, f, tp)
    for t in tp_peers:
        greet(sp, fs, t)

    def greet_sp(d, c):
        greet(lax.rem(sp + d, n_sp), fs, tp)
        return c

    if n_sp <= 8:
        for d in range(1, n_sp):
            greet_sp(d, 0)
    else:
        lax.fori_loop(1, n_sp, greet_sp, 0)

    def col(slot):
        return w_all.at[:, pl.ds(slot * head, head)]

    loads = [
        (tokens, tok_in),
        (in_gain, gain_in),
        (decay_log, decay_in),
        (init_state, init_in),
        (ret_gain, ret_gain_in),
        (diff_lambda, lambda_in),
        (diff_gain, diff_gain_in),
        (ret_query, col(0)),
        (ret_key, col(1)),
        (ret_value, col(2)),
        (diff_value, col(3)),
        (diff_key, w_pair.at[pl.ds(0, head)]),
        (diff_query, w_pair.at[pl.ds(head, head)]),
    ]
    load_copies = [
        pltpu.make_async_copy(src, dst, load_sem.at[i]) for i, (src, dst) in enumerate(loads)
    ]
    for c in load_copies:
        c.start()
    if ring:
        own_wo = pltpu.make_async_copy(out_weight, wo.at[sp], load_sem.at[len(loads)])
        own_wo.start()

    me = fs * n_tp + tp
    own = pl.ds(pl.multiple_of(me * own_rows, own_rows), own_rows)
    load_copies[0].wait()
    load_copies[1].wait()
    wide = tok_in[...].astype(f32)
    scale = lax.rsqrt(jnp.mean(wide * wide, axis=-1, keepdims=True) + EPS)
    x_all[own, :] = (wide * scale * gain_in[...].reshape(1, width)).astype(bf16)

    pl.semaphore_wait(barrier, len(fs_peers) + len(tp_peers) + n_sp - 1)

    cw = width // TOKEN_CHUNKS

    def block(rank, c):
        return x_all.at[
            pl.ds(pl.multiple_of(rank * own_rows, own_rows), own_rows), pl.ds(c * cw, cw)
        ]

    def tok_copy(c, rank, send, f, t):
        return remote(block(rank, c), block(rank, c), send, tok_recv.at[c, rank], sp, f, t)

    pending = []
    for c in range(TOKEN_CHUNKS):
        for i, f in enumerate(fs_peers):
            cp = tok_copy(c, me, tok_send.at[c, i], f, tp)
            cp.start()
            pending.append(cp)
        for i, t in enumerate(tp_peers):
            cp = tok_copy(c, me, fwd_send.at[c, n_fs - 1, i], fs, t)
            cp.start()
            pending.append(cp)

    def wo_copy(origin, way, step):
        src = out_weight if step == 0 else wo.at[origin]
        dest = sp + 1 - 2 * way
        return remote(
            src, wo.at[origin], wo_send.at[way, step], wo_recv.at[origin], dest, fs, tp
        )

    def each_way(step, go):
        for way in range(2):
            origin = sp - step if way == 0 else sp + step
            inside = origin >= 0 if way == 0 else origin < n_sp
            onward = sp < n_sp - 1 if way == 0 else sp > 0

            @pl.when(jnp.logical_and(inside, onward))
            def _():
                go(wo_copy(lax.rem(origin + n_sp, n_sp), way, step))

    def pass_on(step):
        def go(cp):
            if step:
                cp.wait_recv()
            cp.start()

        each_way(step, go)

    if ring:
        pass_on(0)

    load_copies[2].wait()
    d_row = decay_in[...]
    row_at = lax.broadcasted_iota(jnp.int32, (rows, rows), 0)
    col_at = lax.broadcasted_iota(jnp.int32, (rows, rows), 1)
    lower = row_at >= col_at
    d_wide = jnp.broadcast_to(d_row, (rows, rows))
    cum_col = jnp.sum(jnp.where(lower, d_wide, 0.0), axis=1, keepdims=True)
    d_col = jnp.sum(jnp.where(row_at == col_at, d_wide, 0.0), axis=1, keepdims=True)
    cum_row = jnp.sum(jnp.where(row_at <= col_at, d_col, 0.0), axis=0, keepdims=True)
    cum_last = jnp.sum(d_row, axis=1, keepdims=True)
    fade = jnp.exp(jnp.where(lower, cum_col - cum_row, -HUGE)) * head ** (-0.5)
    key_weight = jnp.exp(cum_last - cum_col) * head ** (-0.5)
    query_weight = jnp.exp(cum_col)
    decay = jnp.broadcast_to(jnp.exp(cum_last), (own_rows, head))
    decay_high = decay.astype(bf16).astype(f32)
    first = lax.broadcasted_iota(jnp.int32, (own_rows, head), 0) < own_rows // 2
    st[sp, pl.ds(head, own_rows), :] = jnp.where(first, decay_high, decay - decay_high).astype(bf16)

    for c in load_copies[3:]:
        c.wait()

    total = None
    for c in range(TOKEN_CHUNKS):
        if ring and c == TOKEN_CHUNKS - 1:
            pass_on(1)
        for k, f in enumerate(fs_peers):
            rank = f * n_tp + tp
            tok_copy(c, rank, tok_send.at[c, k], fs, tp).wait_recv()
            for i, t in enumerate(tp_peers):
                cp = tok_copy(c, rank, fwd_send.at[c, k, i], fs, t)
                cp.start()
                pending.append(cp)
        for t in tp_peers:
            for f in [fs] + fs_peers:
                tok_copy(c, f * n_tp + t, tok_send.at[c, 0], fs, tp).wait_recv()
        cols = slice(c * cw, (c + 1) * cw)
        piece = (
            jnp.dot(x_all[:, cols], w_all[cols, :], preferred_element_type=f32),
            lax.dot_general(
                x_all[:, cols],
                w_pair[:, cols],
                (((1,), (1,)), ((), ())),
                preferred_element_type=f32,
            ),
        )
        total = piece if total is None else (total[0] + piece[0], total[1] + piece[1])
    proj, pairs = total[0].astype(bf16), total[1].astype(bf16)
    ret_q, ret_k, ret_v, diff_v = (proj[:, i * head : (i + 1) * head] for i in range(4))
    diff_k, diff_q = pairs[:, :head], pairs[:, head:]
    kv[sp, :, :head] = diff_k
    kv[sp, :, head:] = diff_v

    def to_later(buf, send, recv, go):
        def one(d, c):
            @pl.when(sp + d < n_sp)
            def _():
                cp = remote(buf.at[sp], buf.at[sp], send.at[d], recv.at[sp], sp + d, fs, tp)
                go(cp)

            return c

        if n_sp <= 8:
            for d in range(n_sp - 1, 0, -1):
                one(d, 0)
        else:
            lax.fori_loop(1, n_sp, one, 0)

    to_later(kv, kv_send, kv_recv, lambda cp: cp.start())
    weighted = (ret_k.astype(f32) * key_weight).astype(bf16)
    state = lax.dot_general(
        weighted, ret_v, (((0,), (0,)), ((), ())), preferred_element_type=f32
    )
    st[sp, pl.ds(0, head), :] = state.astype(bf16)
    to_later(st, st_send, st_recv, lambda cp: cp.start())

    scores = lax.dot_general(ret_q, ret_k, (((1,), (1,)), ((), ())), preferred_element_type=f32)
    inner = jnp.dot((scores * fade).astype(bf16), ret_v, preferred_element_type=f32)
    lane = lax.broadcasted_iota(jnp.int32, (rows, 2 * maps), 1)
    zero = jnp.zeros_like(diff_q)
    pair_q = jnp.concatenate(
        [jnp.where(lane < maps, diff_q, zero), jnp.where(lane < maps, zero, diff_q)], axis=0
    )

    def one_block(keys, values, allowed):
        s = lax.dot_general(pair_q, keys, (((1,), (1,)), ((), ())), preferred_element_type=f32)
        s = s * maps ** (-0.5)
        if allowed is not None:
            s = jnp.where(allowed, s, -HUGE)
        peak = jnp.max(s, axis=1, keepdims=True)
        w = jnp.exp(s - peak)
        return (
            peak,
            jnp.sum(w, axis=1, keepdims=True),
            jnp.dot(w.astype(bf16), values, preferred_element_type=f32),
        )

    peak, whole, summed = one_block(diff_k, diff_v, jnp.concatenate([lower, lower], axis=0))

    if ring:
        for step in range(2, n_sp - 1):
            pass_on(step)

    def earlier(d, carry):
        peak, whole, summed, run, entering = carry
        b = sp - d
        remote(kv.at[b], kv.at[b], kv_send.at[0], kv_recv.at[b], sp, fs, tp).wait_recv()
        peak_b, whole_b, sum_b = one_block(kv[b, :, :head], kv[b, :, head:], None)
        top = jnp.maximum(peak, peak_b)
        before, after = jnp.exp(peak - top), jnp.exp(peak_b - top)
        remote(st.at[b], st.at[b], st_send.at[0], st_recv.at[b], sp, fs, tp).wait_recv()
        entering = entering + run * st[b, pl.ds(0, head), :].astype(f32)
        tail = st[b, pl.ds(head, own_rows), :].astype(f32)
        last = own_rows // 2
        return (
            top,
            whole * before + whole_b * after,
            summed * before + sum_b * after,
            run * (tail[0:1] + tail[last : last + 1]),
            entering,
        )

    peak, whole, summed, run, entering = lax.fori_loop(
        1,
        sp + 1,
        earlier,
        (peak, whole, summed, jnp.ones((1, head), f32), jnp.zeros((head, head), f32)),
    )
    entering = entering + run * init_in[0].astype(f32)
    reached = jnp.dot(ret_q, entering.astype(bf16), preferred_element_type=f32)
    ret_out = inner + query_weight * reached
    centre = ret_out - jnp.mean(ret_out, axis=-1, keepdims=True)
    ret_mix = (
        centre
        * lax.rsqrt(jnp.mean(centre * centre, axis=-1, keepdims=True) + EPS)
        * ret_gain_in[...].reshape(1, head)
    ).astype(bf16)
    lam = lambda_in[...].reshape(1, 1)
    ratio = summed / whole
    diff_out = ratio[:rows] - lam * ratio[rows:]
    diff_mix = (
        diff_out
        * lax.rsqrt(jnp.mean(diff_out * diff_out, axis=-1, keepdims=True) + EPS)
        * diff_gain_in[...].reshape(1, head)
    ).astype(bf16)
    mixed = jnp.concatenate([ret_mix, diff_mix], axis=1)

    if ring:
        own_wo.wait()
        order = [sp]
        low, high = sp - 1, sp + 1
        for _ in range(1, n_sp):
            down = jnp.logical_and(
                low >= 0, jnp.logical_or(high >= n_sp, sp - low <= high - sp)
            )
            order.append(jnp.where(down, low, high))
            low, high = jnp.where(down, low - 1, low), jnp.where(down, high, high + 1)
        span = out_weight.shape[2]
    else:
        order = list(range(4))
        span = width // 4

    def columns(s):
        if isinstance(s, int):
            return pl.ds(s * span, span)
        return pl.ds(pl.multiple_of(s * span, 128), span)

    def sib_copy(k, i, t):
        cols = columns(order[k])
        return remote(
            part.at[t, :, cols], sib.at[tp, :, cols], sib_send.at[k, i], sib_recv.at[k, tp], sp, fs, t
        )

    def rs_copy(k, i, f):
        cols = columns(order[k])
        return remote(
            red.at[f, :, cols], rcv.at[fs, :, cols], rs_send.at[k, i], rs_recv.at[k, fs], sp, f, tp
        )

    def reduce_pair(k):
        cols = columns(order[k])
        acc = part[tp, :, cols].astype(f32)
        for i, t in enumerate(tp_peers):
            remote(
                part.at[t, :, cols], sib.at[t, :, cols], sib_send.at[k, i], sib_recv.at[k, t], sp, fs, tp
            ).wait_recv()
            acc = acc + sib[t, :, cols].astype(f32)
        red[:, :, cols] = acc.astype(bf16).reshape(n_fs, own_rows, span)
        for i, f in enumerate(fs_peers):
            cp = rs_copy(k, i, f)
            cp.start()
            pending.append(cp)

    for k, s in enumerate(order):
        if ring and k:

            @pl.when(jnp.logical_or(sp == 0, sp == n_sp - 1))
            def _():
                wo_copy(s, 0, k).wait_recv()

        if ring:
            w = wo[s].reshape(2 * head, span)
        else:
            w = out_weight[:, :, s * span : (s + 1) * span].reshape(2 * head, span)
        value = jnp.dot(mixed, w, preferred_element_type=f32).astype(bf16)
        cols = columns(s)
        for f in range(n_fs):
            for t in range(n_tp):
                at = (f * n_tp + t) * own_rows
                part[t, pl.ds(f * own_rows, own_rows), cols] = value[at : at + own_rows]
        for i, t in enumerate(tp_peers):
            cp = sib_copy(k, i, t)
            cp.start()
            pending.append(cp)
        if k >= 1:
            reduce_pair(k - 1)
    reduce_pair(len(order) - 1)

    for k, s in enumerate(order):
        cols = columns(s)
        acc = red[fs, :, cols].astype(f32)
        for i, f in enumerate(fs_peers):
            remote(
                red.at[f, :, cols], rcv.at[f, :, cols], rs_send.at[k, i], rs_recv.at[k, f], sp, fs, tp
            ).wait_recv()
            acc = acc + rcv[f, :, cols].astype(f32)
        out[:, cols] = acc.astype(bf16)

    for cp in pending:
        cp.wait_send()
    if ring:
        for step in range(n_sp - 1):
            each_way(step, lambda cp: cp.wait_send())
    to_later(kv, kv_send, kv_recv, lambda cp: cp.wait_send())
    to_later(st, st_send, st_recv, lambda cp: cp.wait_send())


def solution(mesh):
    n_sp, n_fs, n_tp = (mesh.shape[a] for a in ("sp", "fs", "tp"))

    def local(*args):
        args = list(args)
        tokens, ret_query, diff_query, out_weight = args[0], args[2], args[8], args[13]
        own_rows, width = tokens.shape
        rows = own_rows * n_fs * n_tp
        head = ret_query.shape[1]
        maps = diff_query.shape[2]
        assert 2 * maps == head
        assert args[5].shape[1] == rows == head
        ring = out_weight.shape[2] % 128 == 0 and 1 < n_sp <= 8
        if not ring:
            args[13] = lax.all_gather(out_weight, "sp", axis=2, tiled=True)
        for i in (8, 9):
            args[i] = jnp.swapaxes(args[i], 1, 2).reshape(2 * maps, width)
        chunks = n_sp if ring else 4
        vmem = pl.BlockSpec(memory_space=pltpu.VMEM)
        hbm = pl.BlockSpec(memory_space=pltpu.HBM)
        in_specs = [hbm] * 13 + [hbm if ring else vmem]
        dma = pltpu.SemaphoreType.DMA
        wo_shape = (n_sp,) + out_weight.shape if ring else (1, 2, 16, 128)
        return pl.pallas_call(
            functools.partial(kernel, (n_sp, n_fs, n_tp, ring)),
            out_shape=jax.ShapeDtypeStruct(tokens.shape, bf16),
            in_specs=in_specs,
            out_specs=vmem,
            scratch_shapes=[
                pltpu.VMEM((rows, width), bf16),
                pltpu.VMEM((width, 4 * head), bf16),
                pltpu.VMEM((4 * maps, width), bf16),
                *[pltpu.VMEM(args[i].shape, args[i].dtype) for i in (0, 1, 5, 6, 7, 11, 12)],
                pltpu.VMEM((n_sp, rows, 2 * head), bf16),
                pltpu.VMEM((n_sp, head + own_rows, head), bf16),
                pltpu.VMEM(wo_shape, bf16),
                pltpu.VMEM((n_tp, n_fs * own_rows, width), bf16),
                pltpu.VMEM((n_tp, n_fs * own_rows, width), bf16),
                pltpu.VMEM((n_fs, own_rows, width), bf16),
                pltpu.VMEM((n_fs, own_rows, width), bf16),
                dma((14,)),
                dma((TOKEN_CHUNKS, n_fs)),
                dma((TOKEN_CHUNKS, n_fs * n_tp)),
                dma((TOKEN_CHUNKS, n_fs, n_tp)),
                dma((n_sp,)),
                dma((n_sp,)),
                dma((n_sp,)),
                dma((n_sp,)),
                dma((2, n_sp)),
                dma((n_sp,)),
                dma((chunks, n_tp)),
                dma((chunks, n_tp)),
                dma((chunks, n_fs)),
                dma((chunks, n_fs)),
            ],
            compiler_params=pltpu.CompilerParams(
                collective_id=0, has_side_effects=True, vmem_limit_bytes=67043328
            ),
            name="layer",
        )(*args)

    in_specs = (
        P(("sp", "fs", "tp"), None),
        P(),
        P(None, ("fs", "tp")),
        P(None, ("fs", "tp")),
        P(None, ("fs", "tp")),
        P(("fs", "tp"), "sp"),
        P(("fs", "tp"), None, None),
        P(("fs", "tp")),
        P(None, None, ("fs", "tp")),
        P(None, None, ("fs", "tp")),
        P(None, ("fs", "tp")),
        P(("fs", "tp")),
        P(("fs", "tp")),
        P(None, ("fs", "tp"), "sp"),
    )
    out_specs = P(("sp", "fs", "tp"), None)
    return jax.shard_map(local, mesh=mesh, in_specs=in_specs, out_specs=out_specs, check_vma=False)
```

profile of v0, /device:TPU:25, one launch (start us, length us, event | category | flops | bytes accessed | tf_op | source)
XLA Modules:
  0.0 37.1 jit_solution(17405451433502923457)
XLA Ops:
  0.7 35.0 %layer.1 = bf16[16,2048]{1,0:T(8,128)(2,1)} custom-call(bf16[16,2048]{1,0:T(8,128)(2,1)} %tokens.1, f32[2048]{0:T(1024)} %in_gain.1, bf16[2048,128]{1,0:T(8,128)(2,1)} %ret_query.1, bf16[2048,128]{1,0:T(8,128)(2,1)} %ret_key.1, bf16[2048,128]{1,0:T(8,128)(2,1)} %ret_value.1, f32[1,128]{1,0:T(1,128)} %decay_log.1, bf16[1,128,128]{2,1,0:T(8,128)(2,1)} %init_state.1, ...), custom_call_target="tpu_custom_call" | custom-call | tf_op jit(solution)/shard_map/layer/pallas_call | solution.py:460
  35.6 1.5 %copy.17 = bf16[16,2048]{1,0:T(8,128)(2,1)} copy(bf16[16,2048]{1,0:T(8,128)(2,1)} %layer.1) | data formatting | bytes 131072
where the time goes:
time: 37.3 us; the launch traced here: 37.1 us
  Pallas kernels  35 us (94%)
  local copies, waits for them, and re-layouts  1.47 us (4%)
  between operations  0.66 us (2%)
    pallas_call x1, Pallas kernels, local(): pl.pallas_call(functools.partial(kernel, (n_sp, n_fs, n_tp, ring)), out_s...  35 us
    unnamed x1, local copies, waits for them, and re-layouts  1.47 us

commit v1 on v0

--- a/solution.py
+++ b/solution.py
@@ -10,6 +10,9 @@
 EPS = 1e-06
 HUGE = 1e30
 TOKEN_CHUNKS = 1
+DIAG = "DDDD"
+FAR = 9
+SEQUENCE = ("c1", "s0", "c2", "d0", "s1", "c3", "p0", "d1", "s2", "p1", "d2", "s3", "d3", "p2", "p3")
 f32 = jnp.float32
 bf16 = jnp.bfloat16
 
@@ -434,6 +437,433 @@
     to_later(st, st_send, st_recv, lambda cp: cp.wait_send())
 
 
+def plane_order(sp, n_sp):
+    return [jnp.where(i <= sp, sp - i, i) for i in range(n_sp)]
+
+
+def gather_plan(n_sp):
+    plan = []
+    for i in range(1, n_sp):
+        plan.append(("own", i))
+    for d in "XYDS" if DIAG[0] == "D" else "XYS":
+        plan.append(("pass", "Z", 0, d))
+
+    def column(i):
+        plan.append(("wait", "Z", i))
+        for d in "XYDS" if DIAG[i] == "D" else "XYS":
+            plan.append(("pass", "Z", i, d))
+
+    def sides(i):
+        for k, other in (("X", "Y"), ("Y", "X")):
+            plan.append(("wait", k, i))
+            if DIAG[i] in (k, "P"):
+                plan.append(("pass", k, i, other))
+            plan.append(("pass", k, i, "S"))
+
+    def corner(i):
+        plan.append(("wait", "D", i))
+        if i == 0:
+            plan.extend(("far", j) for j in range(1, n_sp))
+        plan.append(("pass", "D", i, "S"))
+
+    for step in SEQUENCE:
+        name, i = step[0], int(step[1])
+        if i < n_sp:
+            {"c": column, "s": sides, "d": corner, "p": lambda i: plan.append(("project", i))}[name](i)
+    return plan
+
+
+def whole_kernel(
+    sizes,
+    plan,
+    tokens,
+    in_gain,
+    ret_query,
+    ret_key,
+    ret_value,
+    decay_log,
+    init_state,
+    ret_gain,
+    diff_query,
+    diff_key,
+    diff_value,
+    diff_lambda,
+    diff_gain,
+    out_weight,
+    out,
+    x_all,
+    w_all,
+    w_pair,
+    tok_in,
+    gain_in,
+    decays,
+    init_in,
+    ret_gain_in,
+    lambda_in,
+    diff_gain_in,
+    wo,
+    pair_q,
+    ret_q,
+    ret_k,
+    ret_v,
+    diff_k,
+    diff_v,
+    states,
+    part,
+    sib,
+    red,
+    rcv,
+    fin,
+    got,
+    load_sem,
+    tok_send,
+    tok_recv,
+    decay_send,
+    decay_recv,
+    sib_send,
+    sib_recv,
+    rs_send,
+    rs_recv,
+    fin_send,
+    fin_recv,
+):
+    n_sp, n_fs, n_tp = sizes
+    own_rows, width = tokens.shape
+    rows = own_rows * n_fs * n_tp
+    head = ret_query.shape[1]
+    maps = diff_query.shape[0] // 2
+    span = out_weight.shape[2]
+    sp, fs, tp = lax.axis_index("sp"), lax.axis_index("fs"), lax.axis_index("tp")
+    side = fs + 1 - 2 * lax.rem(fs, 2)
+    ahead = lax.rem(fs + 2, 4)
+    corner = side + ahead - fs
+    mate = 1 - tp
+    chip = {"Z": fs, "X": side, "Y": ahead, "D": corner}
+    order = plane_order(sp, n_sp)
+
+    def remote(src, dst, send, recv, s, f, t):
+        return pltpu.make_async_remote_copy(
+            src_ref=src,
+            dst_ref=dst,
+            send_sem=send,
+            recv_sem=recv,
+            device_id=(s, f, t),
+            device_id_type=pl.DeviceIdType.MESH,
+        )
+
+    barrier = pltpu.get_barrier_semaphore()
+    peers = [(order[i], fs, tp) for i in range(1, n_sp)]
+    peers += [(sp, f, tp) for f in (side, ahead, corner)] + [(sp, fs, mate)]
+    for peer in peers:
+        pl.semaphore_signal(
+            barrier, inc=1, device_id=peer, device_id_type=pl.DeviceIdType.MESH
+        )
+
+    def col(slot):
+        return w_all.at[:, pl.ds(slot * head, head)]
+
+    loads = [
+        (tokens, tok_in),
+        (in_gain, gain_in),
+        (decay_log, decays.at[sp]),
+        (init_state, init_in),
+        (ret_gain, ret_gain_in),
+        (diff_lambda, lambda_in),
+        (diff_gain, diff_gain_in),
+        (ret_query, col(0)),
+        (ret_key, col(1)),
+        (ret_value, col(2)),
+        (diff_value, col(3)),
+        (diff_key, w_pair.at[pl.ds(0, head)]),
+        (diff_query, w_pair.at[pl.ds(head, head)]),
+        (out_weight, wo),
+    ]
+    load_copies = [
+        pltpu.make_async_copy(src, dst, load_sem.at[i]) for i, (src, dst) in enumerate(loads)
+    ]
+    for c in load_copies:
+        c.start()
+    me = (sp * n_fs + fs) * n_tp + tp
+    own = pl.ds(pl.multiple_of(me * own_rows, own_rows), own_rows)
+    load_copies[0].wait()
+    load_copies[1].wait()
+    wide = tok_in[...].astype(f32)
+    scale = lax.rsqrt(jnp.mean(wide * wide, axis=-1, keepdims=True) + EPS)
+    x_all[own, :] = (wide * scale * gain_in[...].reshape(1, width)).astype(bf16)
+    load_copies[2].wait()
+    pl.semaphore_wait(barrier, len(peers))
+
+    pending = []
+
+    def block(k, i, t):
+        rank = (order[i] * n_fs + chip[k]) * n_tp + t
+        return x_all.at[pl.ds(pl.multiple_of(rank * own_rows, own_rows), own_rows)]
+
+    def tok_copy(k, i, t, n, s, f, dest):
+        return remote(block(k, i, t), block(k, i, t), tok_send.at[n], tok_recv.at[order[i], chip[k], t], s, f, dest)
+
+    def send_tok(k, i, s, f, dest, when=None):
+        cp = tok_copy(k, i, tp, len(pending), s, f, dest)
+        pending.append((cp, when))
+        if when is None:
+            cp.start()
+        else:
+            pl.when(when)(cp.start)
+
+    def distant(i):
+        gap = jnp.abs(order[i] - sp)
+        return lax.rem(gap, 2) == 1 if FAR == "odd" else gap >= FAR
+
+    row_at = lax.broadcasted_iota(jnp.int32, (rows, rows), 0)
+    col_at = lax.broadcasted_iota(jnp.int32, (rows, rows), 1)
+    lower = row_at >= col_at
+    lane = lax.broadcasted_iota(jnp.int32, (rows, 2 * maps), 1)
+
+    def cumulate(d_row):
+        d_wide = jnp.broadcast_to(d_row, (rows, rows))
+        return d_wide, jnp.sum(jnp.where(lower, d_wide, 0.0), axis=1, keepdims=True)
+
+    def project(i):
+        p = order[i]
+        for k in "ZXYD":
+            tok_copy(k, i, mate, 0, sp, fs, tp).wait_recv()
+        if i:
+            remote(
+                decays.at[p], decays.at[p], decay_send.at[0], decay_recv.at[p], sp, fs, tp
+            ).wait_recv()
+        else:
+            for c in load_copies[3:]:
+                c.wait()
+        x = x_all[pl.ds(pl.multiple_of(p * rows, rows), rows), :]
+        proj = jnp.dot(x, w_all[...], preferred_element_type=f32).astype(bf16)
+        pairs = lax.dot_general(
+            x, w_pair[...], (((1,), (1,)), ((), ())), preferred_element_type=f32
+        ).astype(bf16)
+        q, k, v, dv = (proj[:, j * head : (j + 1) * head] for j in range(4))
+        dk, dq = pairs[:, :head], pairs[:, head:]
+        zero = jnp.zeros_like(dq)
+        d_row = decays[p]
+        cum_col = cumulate(d_row)[1]
+        cum_last = jnp.sum(d_row, axis=1, keepdims=True)
+        key_weight = jnp.exp(cum_last - cum_col) * head ** (-0.5)
+        states[p] = lax.dot_general(
+            (k.astype(f32) * key_weight).astype(bf16),
+            v,
+            (((0,), (0,)), ((), ())),
+            preferred_element_type=f32,
+        )
+        ret_q[p], ret_k[p], ret_v[p], diff_k[p], diff_v[p] = q, k, v, dk, dv
+        pair_q[p] = jnp.concatenate(
+            [jnp.where(lane < maps, dq, zero), jnp.where(lane < maps, zero, dq)], axis=0
+        )
+
+    fs_peers = [side, ahead, corner]
+
+    def sib_copy(r):
+        return remote(part.at[r, mate], sib.at[r], sib_send.at[r], sib_recv.at[r], sp, fs, mate)
+
+    def rs_copy(r, j):
+        f = fs_peers[j]
+        return remote(red.at[r, f], rcv.at[r, fs], rs_send.at[r, j], rs_recv.at[r, fs], sp, f, tp)
+
+    def fin_copy(r):
+        return remote(fin.at[r], got.at[sp], fin_send.at[r], fin_recv.at[sp], r, fs, tp)
+
+    def finish(r):
+        q, k, v = ret_q[r], ret_k[r], ret_v[r]
+        scores = lax.dot_general(q, k, (((1,), (1,)), ((), ())), preferred_element_type=f32)
+        keys = diff_k[0 : r + 1].reshape((r + 1) * rows, head)
+        s = lax.dot_general(
+            pair_q[r], keys, (((1,), (1,)), ((), ())), preferred_element_type=f32
+        )
+        s = [s[:, b * rows : (b + 1) * rows] for b in range(r + 1)]
+        s[r] = jnp.where(jnp.concatenate([lower, lower], axis=0), s[r], -HUGE)
+        entering = init_in[0].astype(f32)
+        for b in range(r):
+            entering = jnp.exp(jnp.sum(decays[b], axis=1, keepdims=True)) * entering + states[b]
+        reached = jnp.dot(q, entering.astype(bf16), preferred_element_type=f32)
+        d_wide, cum_col = cumulate(decays[r])
+        d_col = jnp.sum(jnp.where(row_at == col_at, d_wide, 0.0), axis=1, keepdims=True)
+        cum_row = jnp.sum(jnp.where(row_at <= col_at, d_col, 0.0), axis=0, keepdims=True)
+        fade = jnp.exp(jnp.where(lower, cum_col - cum_row, -HUGE)) * head ** (-0.5)
+        inner = jnp.dot((scores * fade).astype(bf16), v, preferred_element_type=f32)
+        peak = jnp.max(functools.reduce(jnp.maximum, s), axis=1, keepdims=True)
+        w = [jnp.exp((part_s - peak) * maps ** (-0.5)) for part_s in s]
+        whole = jnp.sum(functools.reduce(jnp.add, w), axis=1, keepdims=True)
+        summed = functools.reduce(
+            jnp.add,
+            [
+                jnp.dot(w[b].astype(bf16), diff_v[b], preferred_element_type=f32)
+                for b in range(r + 1)
+            ],
+        )
+        ret_out = inner + jnp.exp(cum_col) * reached
+        centre = ret_out - jnp.mean(ret_out, axis=-1, keepdims=True)
+        ret_mix = (
+            centre
+            * lax.rsqrt(jnp.mean(centre * centre, axis=-1, keepdims=True) + EPS)
+            * ret_gain_in[...].reshape(1, head)
+        ).astype(bf16)
+        ratio = summed * (1.0 / whole)
+        diff_out = ratio[:rows] - lambda_in[...].reshape(1, 1) * ratio[rows:]
+        diff_mix = (
+            diff_out
+            * lax.rsqrt(jnp.mean(diff_out * diff_out, axis=-1, keepdims=True) + EPS)
+            * diff_gain_in[...].reshape(1, head)
+        ).astype(bf16)
+        mixed = jnp.concatenate([ret_mix, diff_mix], axis=1)
+        value = jnp.dot(mixed, wo[...].reshape(2 * head, span), preferred_element_type=f32).astype(bf16)
+        for f in range(n_fs):
+            for t in range(n_tp):
+                at = (f * n_tp + t) * own_rows
+                part[r, t, pl.ds(f * own_rows, own_rows), :] = value[at : at + own_rows]
+        sib_copy(r).start()
+
+    def reduce_pair(r):
+        sib_copy(r).wait_recv()
+        total = part[r, tp].astype(f32) + sib[r].astype(f32)
+        red[r] = total.astype(bf16).reshape(n_fs, own_rows, span)
+        for j in range(3):
+            rs_copy(r, j).start()
+
+    def collect(r):
+        total = red[r, fs].astype(f32)
+        for f in fs_peers:
+            remote(red.at[r, f], rcv.at[r, f], rs_send.at[r, 0], rs_recv.at[r, f], sp, fs, tp).wait_recv()
+            total = total + rcv[r, f].astype(f32)
+        fin[r] = total.astype(bf16)
+
+        @pl.when(r != sp)
+        def _():
+            fin_copy(r).start()
+
+    def done(i):
+        return 0 if i < 0 else jnp.where(i < sp, 0, i + 1)
+
+    def rows_of(stage, i):
+        def body(r, c):
+            stage(r)
+            return c
+
+        lax.fori_loop(done(i - 1), done(i), body, 0)
+
+    dest = {"X": (sp, side, tp), "Y": (sp, ahead, tp), "D": (sp, corner, tp), "S": (sp, fs, mate)}
+    for step in plan:
+        if step[0] == "own":
+            i = step[1]
+            send_tok("Z", 0, order[i], fs, tp)
+            cp = remote(
+                decays.at[sp], decays.at[sp], decay_send.at[i], decay_recv.at[sp], order[i], fs, tp
+            )
+            cp.start()
+        elif step[0] == "pass":
+            k, i, d = step[1:]
+            cornered = (k == "Z" and d == "D") or (k in "XY" and d in "XY")
+            when = jnp.logical_not(distant(i)) if cornered and i else None
+            if cornered and DIAG[i] == "P":
+                mine = tp == (0 if k == "X" else 1)
+                when = mine if when is None else jnp.logical_and(when, mine)
+            send_tok(k, i, *dest[d], when=when)
+        elif step[0] == "far":
+            send_tok("D", 0, order[step[1]], fs, tp, when=distant(step[1]))
+        elif step[0] == "wait":
+            tok_copy(step[1], step[2], tp, 0, sp, fs, tp).wait_recv()
+        else:
+            i = step[1]
+            project(i)
+            if i:
+                rows_of(reduce_pair, i - 1)
+            if i > 1:
+                rows_of(collect, i - 2)
+            for r in range(i + 1):
+                pl.when(sp <= i if r == i else sp == i)(functools.partial(finish, r))
+                if i == n_sp - 1 and r:
+                    pl.when(sp == i)(functools.partial(reduce_pair, r - 1))
+
+    last = n_sp - 1
+    reduce_pair(last)
+    for cp, when in pending:
+        if when is None:
+            cp.wait_send()
+        else:
+            pl.when(when)(cp.wait_send)
+    rows_of(collect, last - 1)
+    rows_of(collect, last)
+    for c in range(n_sp):
+        cols = slice(c * span, (c + 1) * span)
+
+        @pl.when(sp == c)
+        def _():
+            out[:, cols] = fin[c]
+
+        @pl.when(sp != c)
+        def _():
+            remote(fin.at[c], got.at[c], fin_send.at[0], fin_recv.at[c], sp, fs, tp).wait_recv()
+            out[:, cols] = got[c]
+
+    for i in range(1, n_sp):
+        remote(
+            decays.at[sp], decays.at[sp], decay_send.at[i], decay_recv.at[sp], order[i], fs, tp
+        ).wait_send()
+        fin_copy(order[i]).wait_send()
+    for r in range(n_sp):
+        sib_copy(r).wait_send()
+        for j in range(3):
+            rs_copy(r, j).wait_send()
+
+
+def whole_call(mesh_sizes, args):
+    n_sp, n_fs, n_tp = mesh_sizes
+    tokens, ret_query, diff_query, out_weight = args[0], args[2], args[8], args[13]
+    own_rows, width = tokens.shape
+    rows = own_rows * n_fs * n_tp
+    head = ret_query.shape[1]
+    span = out_weight.shape[2]
+    plan = gather_plan(n_sp)
+    sends = sum(1 for step in plan if step[0] in ("own", "pass", "far"))
+    hbm = pl.BlockSpec(memory_space=pltpu.HBM)
+    dma = pltpu.SemaphoreType.DMA
+    loaded = lambda i: pltpu.VMEM(args[i].shape, args[i].dtype)
+    return pl.pallas_call(
+        functools.partial(whole_kernel, mesh_sizes, plan),
+        out_shape=pltpu.VMEM(tokens.shape, bf16),
+        in_specs=[hbm] * 14,
+        out_specs=pl.BlockSpec(memory_space=pltpu.VMEM),
+        scratch_shapes=[
+            pltpu.VMEM((n_sp * rows, width), bf16),
+            pltpu.VMEM((width, 4 * head), bf16),
+            pltpu.VMEM((2 * head, width), bf16),
+            loaded(0),
+            loaded(1),
+            pltpu.VMEM((n_sp,) + args[5].shape, f32),
+            *[loaded(i) for i in (6, 7, 11, 12)],
+            loaded(13),
+            pltpu.VMEM((n_sp, 2 * rows, head), bf16),
+            *[pltpu.VMEM((n_sp, rows, head), bf16) for _ in range(5)],
+            pltpu.VMEM((n_sp, head, head), f32),
+            pltpu.VMEM((n_sp, n_tp, n_fs * own_rows, span), bf16),
+            pltpu.VMEM((n_sp, n_fs * own_rows, span), bf16),
+            *[pltpu.VMEM((n_sp, n_fs, own_rows, span), bf16) for _ in range(2)],
+            *[pltpu.VMEM((n_sp, own_rows, span), bf16) for _ in range(2)],
+            dma((14,)),
+            dma((sends,)),
+            dma((n_sp, n_fs, n_tp)),
+            dma((n_sp,)),
+            dma((n_sp,)),
+            dma((n_sp,)),
+            dma((n_sp,)),
+            dma((n_sp, 3)),
+            dma((n_sp, n_fs)),
+            dma((n_sp,)),
+            dma((n_sp,)),
+        ],
+        compiler_params=pltpu.CompilerParams(
+            collective_id=0, has_side_effects=True, vmem_limit_bytes=66900000
+        ),
+        name="layer",
+    )(*args)
+
+
 def solution(mesh):
     n_sp, n_fs, n_tp = (mesh.shape[a] for a in ("sp", "fs", "tp"))
 
@@ -447,10 +877,13 @@
         assert 2 * maps == head
         assert args[5].shape[1] == rows == head
         ring = out_weight.shape[2] % 128 == 0 and 1 < n_sp <= 8
+        whole = ring and n_sp <= 4 and n_fs == 4 and n_tp == 2
         if not ring:
             args[13] = lax.all_gather(out_weight, "sp", axis=2, tiled=True)
         for i in (8, 9):
             args[i] = jnp.swapaxes(args[i], 1, 2).reshape(2 * maps, width)
+        if whole:
+            return whole_call((n_sp, n_fs, n_tp), args)
         chunks = n_sp if ring else 4
         vmem = pl.BlockSpec(memory_space=pltpu.VMEM)
         hbm = pl.BlockSpec(memory_space=pltpu.HBM)

time: 37.3 us -> 32.2 us (0.86)
  the two profiles are of different devices: /device:TPU:25 before, /device:TPU:0 now
where the time goes in v1:
time: 32.2 us; the launch traced here: 32 us
  Pallas kernels  30.8 us (96%)
  between operations  0.66 us (2%)
  local copies, waits for them, and re-layouts  0.63 us (2%)
    pallas_call x1, Pallas kernels, whole_call(): pl.pallas_call(functools.partial(whole_kernel, mesh_sizes, plan), out_sha...  30.8 us

profile of v1, /device:TPU:0, one launch (start us, length us, event | category | flops | bytes accessed | tf_op | source)
XLA Modules:
  0.0 32.0 jit_solution(13568932352838801459)
XLA Ops:
  0.7 30.8 %layer.1 = bf16[16,2048]{1,0:T(8,128)(2,1)S(1)} custom-call(bf16[16,2048]{1,0:T(8,128)(2,1)} %tokens.1, f32[2048]{0:T(1024)} %in_gain.1, bf16[2048,128]{1,0:T(8,128)(2,1)} %ret_query.1, bf16[2048,128]{1,0:T(8,128)(2,1)} %ret_key.1, bf16[2048,128]{1,0:T(8,128)(2,1)} %ret_value.1, f32[1,128]{1,0:T(1,128)} %decay_log.1, bf16[1,128,128]{2,1,0:T(8,128)(2,1)} %init_state.1, ...), custom_call_target="tpu_custom_call" | custom-call | tf_op jit(solution)/shard_map/layer/pallas_call | solution.py:827
  31.4 0.6 %copy.16 = bf16[16,2048]{1,0:T(8,128)(2,1)} copy(bf16[16,2048]{1,0:T(8,128)(2,1)S(1)} %layer.1) | data formatting | bytes 131072

commit v2 on v1

--- a/solution.py
+++ b/solution.py
@@ -10,9 +10,7 @@
 EPS = 1e-06
 HUGE = 1e30
 TOKEN_CHUNKS = 1
-DIAG = "DDDD"
-FAR = 9
-SEQUENCE = ("c1", "s0", "c2", "d0", "s1", "c3", "p0", "d1", "s2", "p1", "d2", "s3", "d3", "p2", "p3")
+SEQUENCE = ("c1", "s0", "d0a", "c2b", "d0b", "s1b", "c3b", "c2+a", "s1+a", "c3+a", "p0a", "q0", "c2-a", "s1-a", "c3-a", "d1+", "s2+", "d2+", "p0b", "s3+", "d3+", "d1-", "s2-", "p1", "d2-", "q1", "p2", "s3-", "d3-", "q2", "p3", "q3")
 f32 = jnp.float32
 bf16 = jnp.bfloat16
 
@@ -444,33 +442,69 @@
 def gather_plan(n_sp):
     plan = []
     for i in range(1, n_sp):
-        plan.append(("own", i))
-    for d in "XYDS" if DIAG[0] == "D" else "XYS":
-        plan.append(("pass", "Z", 0, d))
+        plan.append(("", "own", i))
+    for d in "XYDS":
+        plan.append(("", "pass", "Z", 0, d))
 
     def column(i):
         plan.append(("wait", "Z", i))
-        for d in "XYDS" if DIAG[i] == "D" else "XYS":
-            plan.append(("pass", "Z", i, d))
+        plan.extend(("pass", "Z", i, d) for d in "XYDS")
 
     def sides(i):
-        for k, other in (("X", "Y"), ("Y", "X")):
+        for k in "XY":
             plan.append(("wait", k, i))
-            if DIAG[i] in (k, "P"):
-                plan.append(("pass", k, i, other))
             plan.append(("pass", k, i, "S"))
 
     def corner(i):
         plan.append(("wait", "D", i))
-        if i == 0:
-            plan.extend(("far", j) for j in range(1, n_sp))
         plan.append(("pass", "D", i, "S"))
 
     for step in SEQUENCE:
-        name, i = step[0], int(step[1])
-        if i < n_sp:
-            {"c": column, "s": sides, "d": corner, "p": lambda i: plan.append(("project", i))}[name](i)
+        name, i, flags = step[0], int(step[1]), step[2:]
+        begin = len(plan)
+        if name in "pq":
+            plan.append(({"p": "project", "q": "rows"}[name], i))
+        else:
+            {"c": column, "s": sides, "d": corner}[name](i)
+        plan[begin:] = [(flags,) + entry for entry in plan[begin:]]
     return plan
+
+
+def row_plan(n_sp, plane):
+    last = n_sp - 1
+    steps, waiting, late, own = [], [], [], []
+    for i in range(n_sp):
+        ready = list(range(i + 1)) if i == plane else [i] if i > plane else []
+        if plane:
+            ready = [r for r in ready if r]
+        if plane < i == last - 1:
+            late, ready = ready, []
+        elif 0 < i == plane < last - 1:
+            own, ready = ready[-1:], ready[:-1]
+        if i == last:
+            ready = ready + late + own
+        ops, fresh = [], []
+        if plane and i == max(1, plane - 1):
+            ops.append(("borrow", 0))
+        if plane and i == max(1, plane - 1) + 1:
+            ops.append(("reduce", 0))
+        for n, r in enumerate(ready):
+            ops.append(("finish", r))
+            if i == last and n == 0:
+                ops += [("reduce", b) for b in waiting]
+            if fresh and i >= last - 1:
+                ops.append(("reduce", fresh.pop(0)))
+            fresh.append(r)
+        if i == last:
+            if plane:
+                ops.append(("collect", 0))
+            ops += [("reduce", r) for r in fresh]
+            done = [op[1] for step in steps + [ops] for op in step if op[0] == "reduce"]
+            ops += [("collect", r) for r in done if r or not plane]
+        else:
+            waiting += fresh
+        steps.append(ops)
+    return steps
 
 
 def whole_kernel(
@@ -509,6 +543,7 @@
     diff_k,
     diff_v,
     states,
+    mix,
     part,
     sib,
     red,
@@ -518,6 +553,7 @@
     load_sem,
     tok_send,
     tok_recv,
+    mate_recv,
     decay_send,
     decay_recv,
     sib_send,
@@ -526,6 +562,8 @@
     rs_recv,
     fin_send,
     fin_recv,
+    mix_send,
+    mix_recv,
 ):
     n_sp, n_fs, n_tp = sizes
     own_rows, width = tokens.shape
@@ -578,8 +616,14 @@
         (diff_query, w_pair.at[pl.ds(head, head)]),
         (out_weight, wo),
     ]
+    groups = [0, 1, 2, 3, 4, 5, 6, 7, 7, 7, 7, 8, 8, 9]
     load_copies = [
-        pltpu.make_async_copy(src, dst, load_sem.at[i]) for i, (src, dst) in enumerate(loads)
+        pltpu.make_async_copy(src, dst, load_sem.at[i]) for i, (src, dst) in zip(groups, loads)
+    ]
+    later_loads = load_copies[3:7] + [
+        pltpu.make_async_copy(w_all, w_all, load_sem.at[7]),
+        pltpu.make_async_copy(w_pair, w_pair, load_sem.at[8]),
+        load_copies[13],
     ]
     for c in load_copies:
         c.start()
@@ -599,20 +643,22 @@
         rank = (order[i] * n_fs + chip[k]) * n_tp + t
         return x_all.at[pl.ds(pl.multiple_of(rank * own_rows, own_rows), own_rows)]
 
-    def tok_copy(k, i, t, n, s, f, dest):
-        return remote(block(k, i, t), block(k, i, t), tok_send.at[n], tok_recv.at[order[i], chip[k], t], s, f, dest)
-
-    def send_tok(k, i, s, f, dest, when=None):
-        cp = tok_copy(k, i, tp, len(pending), s, f, dest)
-        pending.append((cp, when))
-        if when is None:
-            cp.start()
+    def tok_copy(k, i, s, f, dest):
+        recv = mate_recv.at[order[i]] if dest is mate else tok_recv.at[order[i], chip[k]]
+        return remote(block(k, i, tp), block(k, i, tp), tok_send, recv, s, f, dest)
+
+    tests = {"+": tp == 1, "-": tp == 0, "a": sp == 0, "b": sp > 0}
+
+    def run(flags, go):
+        if flags:
+            pl.when(functools.reduce(jnp.logical_and, [tests[f] for f in flags]))(go)
         else:
-            pl.when(when)(cp.start)
-
-    def distant(i):
-        gap = jnp.abs(order[i] - sp)
-        return lax.rem(gap, 2) == 1 if FAR == "odd" else gap >= FAR
+            go()
+
+    def send_tok(flags, *where):
+        if "-" not in flags and "b" not in flags:
+            pending.append(where)
+        run(flags, tok_copy(*where).start)
 
     row_at = lax.broadcasted_iota(jnp.int32, (rows, rows), 0)
     col_at = lax.broadcasted_iota(jnp.int32, (rows, rows), 1)
@@ -625,14 +671,12 @@
 
     def project(i):
         p = order[i]
-        for k in "ZXYD":
-            tok_copy(k, i, mate, 0, sp, fs, tp).wait_recv()
-        if i:
-            remote(
-                decays.at[p], decays.at[p], decay_send.at[0], decay_recv.at[p], sp, fs, tp
-            ).wait_recv()
-        else:
-            for c in load_copies[3:]:
+        quarter = x_all.at[pl.ds(0, n_fs * own_rows)]
+        remote(quarter, quarter, tok_send, mate_recv.at[p], sp, fs, tp).wait_recv()
+        if i == 1:
+            far_decays.wait_recv()
+        if i == 0:
+            for c in later_loads:
                 c.wait()
         x = x_all[pl.ds(pl.multiple_of(p * rows, rows), rows), :]
         proj = jnp.dot(x, w_all[...], preferred_element_type=f32).astype(bf16)
@@ -660,14 +704,17 @@
     fs_peers = [side, ahead, corner]
 
     def sib_copy(r):
-        return remote(part.at[r, mate], sib.at[r], sib_send.at[r], sib_recv.at[r], sp, fs, mate)
+        return remote(part.at[r, mate], sib.at[r], sib_send, sib_recv.at[r], sp, fs, mate)
+
+    def place(f):
+        return jnp.where(fs > f, fs - 1, fs)
 
     def rs_copy(r, j):
         f = fs_peers[j]
-        return remote(red.at[r, f], rcv.at[r, fs], rs_send.at[r, j], rs_recv.at[r, fs], sp, f, tp)
+        return remote(red.at[r, f], rcv.at[r, place(f)], rs_send.at[r], rs_recv.at[r], sp, f, tp)
 
     def fin_copy(r):
-        return remote(fin.at[r], got.at[sp], fin_send.at[r], fin_recv.at[sp], r, fs, tp)
+        return remote(fin.at[r], got.at[sp], fin_send, fin_recv, r, fs, tp)
 
     def finish(r):
         q, k, v = ret_q[r], ret_k[r], ret_v[r]
@@ -712,6 +759,20 @@
             * diff_gain_in[...].reshape(1, head)
         ).astype(bf16)
         mixed = jnp.concatenate([ret_mix, diff_mix], axis=1)
+        if r == 0:
+            mix[...] = mixed
+            for i in range(1, n_sp):
+                mix_copy(i).start()
+        emit(r, mixed)
+
+    def mix_copy(i):
+        return remote(mix, mix, mix_send.at[i], mix_recv, order[i], fs, tp)
+
+    def borrow(r):
+        mix_copy(0).wait_recv()
+        emit(r, mix[...])
+
+    def emit(r, mixed):
         value = jnp.dot(mixed, wo[...].reshape(2 * head, span), preferred_element_type=f32).astype(bf16)
         for f in range(n_fs):
             for t in range(n_tp):
@@ -727,89 +788,67 @@
             rs_copy(r, j).start()
 
     def collect(r):
+        shares = rcv.at[r]
+        remote(shares, shares, rs_send.at[r], rs_recv.at[r], sp, fs, tp).wait_recv()
         total = red[r, fs].astype(f32)
-        for f in fs_peers:
-            remote(red.at[r, f], rcv.at[r, f], rs_send.at[r, 0], rs_recv.at[r, f], sp, fs, tp).wait_recv()
-            total = total + rcv[r, f].astype(f32)
+        for j in range(n_fs - 1):
+            total = total + rcv[r, j].astype(f32)
         fin[r] = total.astype(bf16)
 
         @pl.when(r != sp)
         def _():
             fin_copy(r).start()
 
-    def done(i):
-        return 0 if i < 0 else jnp.where(i < sp, 0, i + 1)
-
-    def rows_of(stage, i):
-        def body(r, c):
-            stage(r)
-            return c
-
-        lax.fori_loop(done(i - 1), done(i), body, 0)
-
     dest = {"X": (sp, side, tp), "Y": (sp, ahead, tp), "D": (sp, corner, tp), "S": (sp, fs, mate)}
-    for step in plan:
-        if step[0] == "own":
-            i = step[1]
-            send_tok("Z", 0, order[i], fs, tp)
-            cp = remote(
-                decays.at[sp], decays.at[sp], decay_send.at[i], decay_recv.at[sp], order[i], fs, tp
-            )
-            cp.start()
-        elif step[0] == "pass":
-            k, i, d = step[1:]
-            cornered = (k == "Z" and d == "D") or (k in "XY" and d in "XY")
-            when = jnp.logical_not(distant(i)) if cornered and i else None
-            if cornered and DIAG[i] == "P":
-                mine = tp == (0 if k == "X" else 1)
-                when = mine if when is None else jnp.logical_and(when, mine)
-            send_tok(k, i, *dest[d], when=when)
-        elif step[0] == "far":
-            send_tok("D", 0, order[step[1]], fs, tp, when=distant(step[1]))
-        elif step[0] == "wait":
-            tok_copy(step[1], step[2], tp, 0, sp, fs, tp).wait_recv()
+    stages = {"finish": finish, "borrow": borrow, "reduce": reduce_pair, "collect": collect}
+    row_plans = [row_plan(n_sp, plane) for plane in range(n_sp)]
+
+    all_decays = decays.at[pl.ds(0, n_sp - 1)]
+    far_decays = remote(all_decays, all_decays, decay_send, decay_recv, sp, fs, tp)
+    for flags, kind, *step in plan:
+        if kind == "own":
+            i = step[0]
+            send_tok(flags, "Z", 0, order[i], fs, tp)
+            remote(
+                decays.at[sp], decays.at[sp], decay_send, decay_recv, order[i], fs, tp
+            ).start()
+        elif kind == "pass":
+            send_tok(flags, *step[:2], *dest[step[2]])
+        elif kind == "wait":
+            run(flags, tok_copy(*step, sp, fs, tp).wait_recv)
+        elif kind == "project":
+            run(flags, functools.partial(project, step[0]))
         else:
-            i = step[1]
-            project(i)
-            if i:
-                rows_of(reduce_pair, i - 1)
-            if i > 1:
-                rows_of(collect, i - 2)
-            for r in range(i + 1):
-                pl.when(sp <= i if r == i else sp == i)(functools.partial(finish, r))
-                if i == n_sp - 1 and r:
-                    pl.when(sp == i)(functools.partial(reduce_pair, r - 1))
-
-    last = n_sp - 1
-    reduce_pair(last)
-    for cp, when in pending:
-        if when is None:
-            cp.wait_send()
-        else:
-            pl.when(when)(cp.wait_send)
-    rows_of(collect, last - 1)
-    rows_of(collect, last)
+            i = step[0]
+            for plane in range(n_sp):
+
+                def rows_done(ops=row_plans[plane][i]):
+                    for stage, r in ops:
+                        stages[stage](r)
+
+                if row_plans[plane][i]:
+                    pl.when(sp == plane)(rows_done)
+
+    others = got.at[pl.ds(0, n_sp - 1)]
+    arrived = remote(others, others, fin_send, fin_recv, sp, fs, tp)
+    arrived.wait_recv()
     for c in range(n_sp):
-        cols = slice(c * span, (c + 1) * span)
-
-        @pl.when(sp == c)
-        def _():
-            out[:, cols] = fin[c]
-
-        @pl.when(sp != c)
-        def _():
-            remote(fin.at[c], got.at[c], fin_send.at[0], fin_recv.at[c], sp, fs, tp).wait_recv()
-            out[:, cols] = got[c]
-
-    for i in range(1, n_sp):
-        remote(
-            decays.at[sp], decays.at[sp], decay_send.at[i], decay_recv.at[sp], order[i], fs, tp
-        ).wait_send()
-        fin_copy(order[i]).wait_send()
+        out[:, c * span : (c + 1) * span] = jnp.where(sp == c, fin[c], got[c])
+
+    sent = x_all.at[pl.ds(0, len(pending) * own_rows)]
+    remote(sent, sent, tok_send, mate_recv.at[0], sp, fs, tp).wait_send()
+    far_decays.wait_send()
+    halves = part.at[:, 0]
+    remote(halves, halves, sib_send, sib_recv.at[0], sp, fs, tp).wait_send()
     for r in range(n_sp):
-        sib_copy(r).wait_send()
-        for j in range(3):
-            rs_copy(r, j).wait_send()
+        shares = rcv.at[r]
+        remote(shares, shares, rs_send.at[r], rs_recv.at[r], sp, fs, tp).wait_send()
+    arrived.wait_send()
+
+    @pl.when(sp == 0)
+    def _():
+        for i in range(1, n_sp):
+            mix_copy(i).wait_send()
 
 
 def whole_call(mesh_sizes, args):
@@ -820,7 +859,6 @@
     head = ret_query.shape[1]
     span = out_weight.shape[2]
     plan = gather_plan(n_sp)
-    sends = sum(1 for step in plan if step[0] in ("own", "pass", "far"))
     hbm = pl.BlockSpec(memory_space=pltpu.HBM)
     dma = pltpu.SemaphoreType.DMA
     loaded = lambda i: pltpu.VMEM(args[i].shape, args[i].dtype)
@@ -841,21 +879,26 @@
             pltpu.VMEM((n_sp, 2 * rows, head), bf16),
             *[pltpu.VMEM((n_sp, rows, head), bf16) for _ in range(5)],
             pltpu.VMEM((n_sp, head, head), f32),
+            pltpu.VMEM((rows, 2 * head), bf16),
             pltpu.VMEM((n_sp, n_tp, n_fs * own_rows, span), bf16),
             pltpu.VMEM((n_sp, n_fs * own_rows, span), bf16),
-            *[pltpu.VMEM((n_sp, n_fs, own_rows, span), bf16) for _ in range(2)],
+            pltpu.VMEM((n_sp, n_fs, own_rows, span), bf16),
+            pltpu.VMEM((n_sp, n_fs - 1, own_rows, span), bf16),
             *[pltpu.VMEM((n_sp, own_rows, span), bf16) for _ in range(2)],
-            dma((14,)),
-            dma((sends,)),
-            dma((n_sp, n_fs, n_tp)),
+            dma((10,)),
+            dma,
+            dma((n_sp, n_fs)),
+            dma((n_sp,)),
+            dma,
+            dma,
+            dma,
             dma((n_sp,)),
             dma((n_sp,)),
             dma((n_sp,)),
+            dma,
+            dma,
             dma((n_sp,)),
-            dma((n_sp, 3)),
-            dma((n_sp, n_fs)),
-            dma((n_sp,)),
-            dma((n_sp,)),
+            dma,
         ],
         compiler_params=pltpu.CompilerParams(
             collective_id=0, has_side_effects=True, vmem_limit_bytes=66900000
@@ -877,7 +920,7 @@
         assert 2 * maps == head
         assert args[5].shape[1] == rows == head
         ring = out_weight.shape[2] % 128 == 0 and 1 < n_sp <= 8
-        whole = ring and n_sp <= 4 and n_fs == 4 and n_tp == 2
+        whole = ring and n_sp == 4 and n_fs == 4 and n_tp == 2
         if not ring:
             args[13] = lax.all_gather(out_weight, "sp", axis=2, tiled=True)
         for i in (8, 9):

time: 32.2 us -> 31 us (0.963)
  Pallas kernels: 30.8 us -> 29.6 us
    pallas_call x1, Pallas kernels: 30.8 us -> 29.6 us  [whole_call(): pl.pallas_call(functools.partial(whole_kernel, mesh_sizes, plan), out_sha...]
where the time goes in v2:
time: 31 us; the launch traced here: 30.9 us
  Pallas kernels  29.6 us (95%)
  between operations  0.66 us (2%)
  local copies, waits for them, and re-layouts  0.63 us (2%)
    pallas_call x1, Pallas kernels, whole_call(): pl.pallas_call(functools.partial(whole_kernel, mesh_sizes, plan), out_sha...  29.6 us
    unnamed x1, local copies, waits for them, and re-layouts  0.63 us

profile of v2, /device:TPU:0, one launch (start us, length us, event | category | flops | bytes accessed | tf_op | source)
XLA Modules:
  0.0 30.9 jit_solution(4817483435722590374)
XLA Ops:
  0.7 29.6 %layer.1 = bf16[16,2048]{1,0:T(8,128)(2,1)S(1)} custom-call(bf16[16,2048]{1,0:T(8,128)(2,1)} %tokens.1, f32[2048]{0:T(1024)} %in_gain.1, bf16[2048,128]{1,0:T(8,128)(2,1)} %ret_query.1, bf16[2048,128]{1,0:T(8,128)(2,1)} %ret_key.1, bf16[2048,128]{1,0:T(8,128)(2,1)} %ret_value.1, f32[1,128]{1,0:T(1,128)} %decay_log.1, bf16[1,128,128]{2,1,0:T(8,128)(2,1)} %init_state.1, ...), custom_call_target="tpu_custom_call" | custom-call | tf_op jit(solution)/shard_map/layer/pallas_call | solution.py:865
  30.3 0.6 %copy.16 = bf16[16,2048]{1,0:T(8,128)(2,1)} copy(bf16[16,2048]{1,0:T(8,128)(2,1)S(1)} %layer.1) | data formatting | bytes 131072

commit v3 on v2

--- a/solution.py
+++ b/solution.py
@@ -10,7 +10,8 @@
 EPS = 1e-06
 HUGE = 1e30
 TOKEN_CHUNKS = 1
-SEQUENCE = ("c1", "s0", "d0a", "c2b", "d0b", "s1b", "c3b", "c2+a", "s1+a", "c3+a", "p0a", "q0", "c2-a", "s1-a", "c3-a", "d1+", "s2+", "d2+", "p0b", "s3+", "d3+", "d1-", "s2-", "p1", "d2-", "q1", "p2", "s3-", "d3-", "q2", "p3", "q3")
+DOWN = True
+SEQUENCE = ("c1", "s0", "d0", "c2b", "s1b", "c3b", "c2+a", "s1+a", "c3+a", "p0a", "q0", "c2-a", "s1-a", "c3-a", "d1+", "s2+", "d2+", "s3+", "d3+", "p0b", "d1-a", "s2-a", "d2-a", "d3-a", "d1-b", "s2-b", "p1", "d2-b", "s3-a", "q1", "p2", "s3-b", "d3-b", "q2", "p3", "q3")
 f32 = jnp.float32
 bf16 = jnp.bfloat16
 
@@ -448,7 +449,8 @@
 
     def column(i):
         plan.append(("wait", "Z", i))
-        plan.extend(("pass", "Z", i, d) for d in "XYDS")
+        plan.extend(("pass", "Z", i, d) for d in "XYS")
+        plan.append(("corner", i))
 
     def sides(i):
         for k in "XY":
@@ -457,6 +459,8 @@
 
     def corner(i):
         plan.append(("wait", "D", i))
+        if i == 0 and DOWN:
+            plan.append(("down",))
         plan.append(("pass", "D", i, "S"))
 
     for step in SEQUENCE:
@@ -484,10 +488,11 @@
         if i == last:
             ready = ready + late + own
         ops, fresh = [], []
-        if plane and i == max(1, plane - 1):
+        if plane and i == last - 1:
             ops.append(("borrow", 0))
-        if plane and i == max(1, plane - 1) + 1:
-            ops.append(("reduce", 0))
+            fresh.append(0)
+        if plane == last == i:
+            ops.append(("reduce", waiting.pop()))
         for n, r in enumerate(ready):
             ops.append(("finish", r))
             if i == last and n == 0:
@@ -637,7 +642,7 @@
     load_copies[2].wait()
     pl.semaphore_wait(barrier, len(peers))
 
-    pending = []
+    pending = {}
 
     def block(k, i, t):
         rank = (order[i] * n_fs + chip[k]) * n_tp + t
@@ -656,8 +661,10 @@
             go()
 
     def send_tok(flags, *where):
-        if "-" not in flags and "b" not in flags:
-            pending.append(where)
+        if "-" not in flags:
+            for kind in "ab":
+                if kind in flags or not set("ab") & set(flags):
+                    pending[kind] = pending.get(kind, 0) + 1
         run(flags, tok_copy(*where).start)
 
     row_at = lax.broadcasted_iota(jnp.int32, (rows, rows), 0)
@@ -761,7 +768,7 @@
         mixed = jnp.concatenate([ret_mix, diff_mix], axis=1)
         if r == 0:
             mix[...] = mixed
-            for i in range(1, n_sp):
+            for i in range(n_sp - 1, 0, -1):
                 mix_copy(i).start()
         emit(r, mixed)
 
@@ -814,6 +821,12 @@
             ).start()
         elif kind == "pass":
             send_tok(flags, *step[:2], *dest[step[2]])
+        elif kind == "corner":
+            if not (DOWN and "a" in flags):
+                send_tok(flags + ("b" if DOWN and "b" not in flags else ""), "Z", step[0], *dest["D"])
+        elif kind == "down":
+            if "a" not in flags:
+                send_tok(flags + ("" if "b" in flags else "b"), "D", 0, 0, fs, tp)
         elif kind == "wait":
             run(flags, tok_copy(*step, sp, fs, tp).wait_recv)
         elif kind == "project":
@@ -835,8 +848,9 @@
     for c in range(n_sp):
         out[:, c * span : (c + 1) * span] = jnp.where(sp == c, fin[c], got[c])
 
-    sent = x_all.at[pl.ds(0, len(pending) * own_rows)]
-    remote(sent, sent, tok_send, mate_recv.at[0], sp, fs, tp).wait_send()
+    for flag, count in pending.items():
+        sent = x_all.at[pl.ds(0, count * own_rows)]
+        run(flag, remote(sent, sent, tok_send, mate_recv.at[0], sp, fs, tp).wait_send)
     far_decays.wait_send()
     halves = part.at[:, 0]
     remote(halves, halves, sib_send, sib_recv.at[0], sp, fs, tp).wait_send()

time: 31 us -> 30 us (0.968)
  Pallas kernels: 29.6 us -> 28.6 us
    pallas_call x1, Pallas kernels: 29.6 us -> 28.6 us  [whole_call(): pl.pallas_call(functools.partial(whole_kernel, mesh_sizes, plan), out_sha...]
where the time goes in v3:
time: 30 us; the launch traced here: 29.9 us
  Pallas kernels  28.6 us (95%)
  between operations  0.66 us (2%)
  local copies, waits for them, and re-layouts  0.63 us (2%)
    pallas_call x1, Pallas kernels, whole_call(): pl.pallas_call(functools.partial(whole_kernel, mesh_sizes, plan), out_sha...  28.6 us
    unnamed x1, local copies, waits for them, and re-layouts  0.63 us

profile of v3, /device:TPU:0, one launch (start us, length us, event | category | flops | bytes accessed | tf_op | source)
XLA Modules:
  0.0 29.9 jit_solution(13884511238233481334)
XLA Ops:
  0.7 28.6 %layer.1 = bf16[16,2048]{1,0:T(8,128)(2,1)S(1)} custom-call(bf16[16,2048]{1,0:T(8,128)(2,1)} %tokens.1, f32[2048]{0:T(1024)} %in_gain.1, bf16[2048,128]{1,0:T(8,128)(2,1)} %ret_query.1, bf16[2048,128]{1,0:T(8,128)(2,1)} %ret_key.1, bf16[2048,128]{1,0:T(8,128)(2,1)} %ret_value.1, f32[1,128]{1,0:T(1,128)} %decay_log.1, bf16[1,128,128]{2,1,0:T(8,128)(2,1)} %init_state.1, ...), custom_call_target="tpu_custom_call" | custom-call | tf_op jit(solution)/shard_map/layer/pallas_call | solution.py:879
  29.3 0.6 %copy.16 = bf16[16,2048]{1,0:T(8,128)(2,1)} copy(bf16[16,2048]{1,0:T(8,128)(2,1)S(1)} %layer.1) | data formatting | bytes 131072

commit v4 on v3

--- a/solution.py
+++ b/solution.py
@@ -10,8 +10,9 @@
 EPS = 1e-06
 HUGE = 1e30
 TOKEN_CHUNKS = 1
-DOWN = True
-SEQUENCE = ("c1", "s0", "d0", "c2b", "s1b", "c3b", "c2+a", "s1+a", "c3+a", "p0a", "q0", "c2-a", "s1-a", "c3-a", "d1+", "s2+", "d2+", "s3+", "d3+", "p0b", "d1-a", "s2-a", "d2-a", "d3-a", "d1-b", "s2-b", "p1", "d2-b", "s3-a", "q1", "p2", "s3-b", "d3-b", "q2", "p3", "q3")
+DOWN = 2
+EARLY = True
+SEQUENCE = ("c1", "s0", "d0", "c2b", "s1b", "c3b", "c2+a", "s1+a", "c3+a", "p0a", "q0", "c2-a", "s1-a", "c3-a", "d1+", "s2+", "d2+", "s3+", "d3+", "p0b", "d1-a", "p1a", "s2-a", "d2-a", "d3-a", "q1", "s3-a", "d1-b", "s2-b", "p1b", "d2-b", "p2", "s3-b", "d3-b", "q2", "p3", "q3")
 f32 = jnp.float32
 bf16 = jnp.bfloat16
 
@@ -459,7 +460,7 @@
 
     def corner(i):
         plan.append(("wait", "D", i))
-        if i == 0 and DOWN:
+        if i == 0:
             plan.append(("down",))
         plan.append(("pass", "D", i, "S"))
 
@@ -491,7 +492,7 @@
         if plane and i == last - 1:
             ops.append(("borrow", 0))
             fresh.append(0)
-        if plane == last == i:
+        if plane == last == i or (EARLY and plane == 0 and i == 1):
             ops.append(("reduce", waiting.pop()))
         for n, r in enumerate(ready):
             ops.append(("finish", r))
@@ -642,7 +643,7 @@
     load_copies[2].wait()
     pl.semaphore_wait(barrier, len(peers))
 
-    pending = {}
+    pending = [0] * n_sp
 
     def block(k, i, t):
         rank = (order[i] * n_fs + chip[k]) * n_tp + t
@@ -652,7 +653,8 @@
         recv = mate_recv.at[order[i]] if dest is mate else tok_recv.at[order[i], chip[k]]
         return remote(block(k, i, tp), block(k, i, tp), tok_send, recv, s, f, dest)
 
-    tests = {"+": tp == 1, "-": tp == 0, "a": sp == 0, "b": sp > 0}
+    tests = {"+": tp == 1, "-": tp == 0, "a": sp == 0, "b": sp > 0, "h": sp >= DOWN}
+    least = {"b": 1, "h": DOWN}
 
     def run(flags, go):
         if flags:
@@ -662,9 +664,9 @@
 
     def send_tok(flags, *where):
         if "-" not in flags:
-            for kind in "ab":
-                if kind in flags or not set("ab") & set(flags):
-                    pending[kind] = pending.get(kind, 0) + 1
+            for plane in range(n_sp):
+                if plane >= max(least.get(f, 0) for f in flags + "+") and not ("a" in flags and plane):
+                    pending[plane] += 1
         run(flags, tok_copy(*where).start)
 
     row_at = lax.broadcasted_iota(jnp.int32, (rows, rows), 0)
@@ -708,7 +710,7 @@
             [jnp.where(lane < maps, dq, zero), jnp.where(lane < maps, zero, dq)], axis=0
         )
 
-    fs_peers = [side, ahead, corner]
+    fs_peers = [corner, side, ahead]
 
     def sib_copy(r):
         return remote(part.at[r, mate], sib.at[r], sib_send, sib_recv.at[r], sp, fs, mate)
@@ -822,11 +824,12 @@
         elif kind == "pass":
             send_tok(flags, *step[:2], *dest[step[2]])
         elif kind == "corner":
-            if not (DOWN and "a" in flags):
-                send_tok(flags + ("b" if DOWN and "b" not in flags else ""), "Z", step[0], *dest["D"])
+            far = step[0] >= DOWN
+            if not (far and "a" in flags):
+                send_tok(flags + "b" * (far and "b" not in flags), "Z", step[0], *dest["D"])
         elif kind == "down":
             if "a" not in flags:
-                send_tok(flags + ("" if "b" in flags else "b"), "D", 0, 0, fs, tp)
+                send_tok(flags + "h", "D", 0, 0, fs, tp)
         elif kind == "wait":
             run(flags, tok_copy(*step, sp, fs, tp).wait_recv)
         elif kind == "project":
@@ -848,9 +851,11 @@
     for c in range(n_sp):
         out[:, c * span : (c + 1) * span] = jnp.where(sp == c, fin[c], got[c])
 
-    for flag, count in pending.items():
+    for plane, count in enumerate(pending):
         sent = x_all.at[pl.ds(0, count * own_rows)]
-        run(flag, remote(sent, sent, tok_send, mate_recv.at[0], sp, fs, tp).wait_send)
+        pl.when(sp == plane)(
+            remote(sent, sent, tok_send, mate_recv.at[0], sp, fs, tp).wait_send
+        )
     far_decays.wait_send()
     halves = part.at[:, 0]
     remote(halves, halves, sib_send, sib_recv.at[0], sp, fs, tp).wait_send()

time: 30 us -> 29.4 us (0.980)
  Pallas kernels: 28.6 us -> 28 us
    pallas_call x1, Pallas kernels: 28.6 us -> 28 us  [whole_call(): pl.pallas_call(functools.partial(whole_kernel, mesh_sizes, plan), out_sha...]
where the time goes in v4:
time: 29.4 us; the launch traced here: 29.3 us
  Pallas kernels  28 us (95%)
  between operations  0.66 us (2%)
  local copies, waits for them, and re-layouts  0.63 us (2%)
    pallas_call x1, Pallas kernels, whole_call(): pl.pallas_call(functools.partial(whole_kernel, mesh_sizes, plan), out_sha...  28 us
    unnamed x1, local copies, waits for them, and re-layouts  0.63 us

profile of v4, /device:TPU:0, one launch (start us, length us, event | category | flops | bytes accessed | tf_op | source)
XLA Modules:
  0.0 29.3 jit_solution(13872376095131453286)
XLA Ops:
  0.7 28.0 %layer.1 = bf16[16,2048]{1,0:T(8,128)(2,1)S(1)} custom-call(bf16[16,2048]{1,0:T(8,128)(2,1)} %tokens.1, f32[2048]{0:T(1024)} %in_gain.1, bf16[2048,128]{1,0:T(8,128)(2,1)} %ret_query.1, bf16[2048,128]{1,0:T(8,128)(2,1)} %ret_key.1, bf16[2048,128]{1,0:T(8,128)(2,1)} %ret_value.1, f32[1,128]{1,0:T(1,128)} %decay_log.1, bf16[1,128,128]{2,1,0:T(8,128)(2,1)} %init_state.1, ...), custom_call_target="tpu_custom_call" | custom-call | tf_op jit(solution)/shard_map/layer/pallas_call | solution.py:884
  28.6 0.6 %copy.16 = bf16[16,2048]{1,0:T(8,128)(2,1)} copy(bf16[16,2048]{1,0:T(8,128)(2,1)S(1)} %layer.1) | data formatting | bytes 131072

commit v5 on v4

--- a/solution.py
+++ b/solution.py
@@ -12,7 +12,7 @@
 TOKEN_CHUNKS = 1
 DOWN = 2
 EARLY = True
-SEQUENCE = ("c1", "s0", "d0", "c2b", "s1b", "c3b", "c2+a", "s1+a", "c3+a", "p0a", "q0", "c2-a", "s1-a", "c3-a", "d1+", "s2+", "d2+", "s3+", "d3+", "p0b", "d1-a", "p1a", "s2-a", "d2-a", "d3-a", "q1", "s3-a", "d1-b", "s2-b", "p1b", "d2-b", "p2", "s3-b", "d3-b", "q2", "p3", "q3")
+SEQUENCE = ("c1", "s0", "d0", "c2b", "s1b", "c3b", "c2+a", "s1+a", "c3+a", "p0a", "q0", "c2-a", "s1-a", "c3-a", "d1+", "s2+", "d2+", "s3+", "d3+", "p0b", "d1-a", "p1a", "s2-a", "d2-a", "d3-a", "q1", "s3-a", "d1-b", "s2-b", "p1b", "d2-b", "m0+f", "p2", "s3-b", "d3-b", "q2", "p3", "q3")
 f32 = jnp.float32
 bf16 = jnp.bfloat16
 
@@ -467,8 +467,8 @@
     for step in SEQUENCE:
         name, i, flags = step[0], int(step[1]), step[2:]
         begin = len(plan)
-        if name in "pq":
-            plan.append(({"p": "project", "q": "rows"}[name], i))
+        if name in "pqm":
+            plan.append(({"p": "project", "q": "rows", "m": "borrow"}[name], i))
         else:
             {"c": column, "s": sides, "d": corner}[name](i)
         plan[begin:] = [(flags,) + entry for entry in plan[begin:]]
@@ -653,7 +653,7 @@
         recv = mate_recv.at[order[i]] if dest is mate else tok_recv.at[order[i], chip[k]]
         return remote(block(k, i, tp), block(k, i, tp), tok_send, recv, s, f, dest)
 
-    tests = {"+": tp == 1, "-": tp == 0, "a": sp == 0, "b": sp > 0, "h": sp >= DOWN}
+    tests = {"+": tp == 1, "-": tp == 0, "a": sp == 0, "b": sp > 0, "h": sp >= DOWN, "f": sp > 1}
     least = {"b": 1, "h": DOWN}
 
     def run(flags, go):
@@ -834,13 +834,18 @@
             run(flags, tok_copy(*step, sp, fs, tp).wait_recv)
         elif kind == "project":
             run(flags, functools.partial(project, step[0]))
+        elif kind == "borrow":
+            run(flags, functools.partial(borrow, 0))
         else:
             i = step[0]
             for plane in range(n_sp):
 
-                def rows_done(ops=row_plans[plane][i]):
+                def rows_done(ops=row_plans[plane][i], plane=plane):
                     for stage, r in ops:
-                        stages[stage](r)
+                        if stage == "borrow" and plane > 1:
+                            run("-", functools.partial(borrow, r))
+                        else:
+                            stages[stage](r)
 
                 if row_plans[plane][i]:
                     pl.when(sp == plane)(rows_done)

time: 29.4 us -> 29.2 us (level)
  no operation moved by 1% of the time
where the time goes in v5:
time: 29.2 us; the launch traced here: 29.1 us
  Pallas kernels  27.8 us (95%)
  between operations  0.66 us (2%)
  local copies, waits for them, and re-layouts  0.63 us (2%)
    pallas_call x1, Pallas kernels, whole_call(): pl.pallas_call(functools.partial(whole_kernel, mesh_sizes, plan), out_sha...  27.8 us
    unnamed x1, local copies, waits for them, and re-layouts  0.63 us

profile of v5, /device:TPU:0, one launch (start us, length us, event | category | flops | bytes accessed | tf_op | source)
XLA Modules:
  0.0 29.1 jit_solution(851632995328661289)
XLA Ops:
  0.7 27.8 %layer.1 = bf16[16,2048]{1,0:T(8,128)(2,1)S(1)} custom-call(bf16[16,2048]{1,0:T(8,128)(2,1)} %tokens.1, f32[2048]{0:T(1024)} %in_gain.1, bf16[2048,128]{1,0:T(8,128)(2,1)} %ret_query.1, bf16[2048,128]{1,0:T(8,128)(2,1)} %ret_key.1, bf16[2048,128]{1,0:T(8,128)(2,1)} %ret_value.1, f32[1,128]{1,0:T(1,128)} %decay_log.1, bf16[1,128,128]{2,1,0:T(8,128)(2,1)} %init_state.1, ...), custom_call_target="tpu_custom_call" | custom-call | tf_op jit(solution)/shard_map/layer/pallas_call | solution.py:889
  28.4 0.6 %copy.16 = bf16[16,2048]{1,0:T(8,128)(2,1)} copy(bf16[16,2048]{1,0:T(8,128)(2,1)S(1)} %layer.1) | data formatting | bytes 131072
